TPU v7x, 32 devices: a whole 2x2x4 slice. The times are simulated.
32 devices in a mesh: sp: 4 (over z), dp: 8 (over y, x, core).
Axes of the slice: x: 2, y: 2, z: 4, core: 2. Of those that a mesh axis runs over, the one named last changes fastest.
Arguments:
- normed: bfloat16 [8, 1024, 512], P('dp', None, 'sp'), may hold values from -6 to 6
- branch_in: bfloat16 [8, 1024, 512], P('dp', 'sp'), may hold values from -12 to 12
- gate_pre: bfloat16 [8, 1024, 512], P('dp', 'sp'), may hold values from -6 to 6
- cotangent: bfloat16 [8, 1024, 512], P('dp', None, 'sp'), may hold values from -6 to 6
- decay_shift: float32 [8, 16, 512], P('dp', 'sp'), may hold values from -1.2 to -0.000390625
- conv_weight: float32 [4, 1024], P(None, 'sp'), may hold values from -3 to 3
- recur_weight: float32 [16, 64, 64], P('sp'), may hold values from -0.75 to 0.75
- input_weight: float32 [16, 64, 64], P('sp'), may hold values from -0.75 to 0.75
- decay_param: float32 [1024], P('sp')
- branch_proj: bfloat16 [1024, 1024], P('dp'), may hold values from -0.1875 to 0.1875
Outputs:
- grad_normed: bfloat16 [8, 1024, 512], P('dp', None, 'sp')
- grad_gate: bfloat16 [8, 1024, 512], P('dp', 'sp')
- grad_proj: float32 [1024, 1024], P('dp', 'sp')
- grad_conv: float32 [4, 1024], P(None, 'sp')
- grad_recur: float32 [16, 64, 64], P('sp')
- grad_input: float32 [16, 64, 64], P('sp')
- grad_decay: float32 [1024], P('sp')
All inputs are finite; a program needn't handle non-finite values.
Results may differ from a plain program's by a relative error of at most 0.019.
Values may be sent and summed in bfloat16 or wider, within the bound.
A program may use at most 64 MiB of HBM per device.

v0:
```python
import math
import jax
import jax.numpy as jnp
from jax import lax
from jax.sharding import PartitionSpec as P

BLOCK_W = 64
CONV = 4
gate_const = 8.0
highest = lax.Precision.HIGHEST
far_below = -1e30


def block_states(log_decay, pushed):
    channels, length = pushed.shape
    span_len = math.gcd(length, 128)
    count = length // span_len
    logs = log_decay.reshape(channels, count, span_len).transpose(1, 0, 2)
    inputs = pushed.reshape(channels, count, span_len).transpose(1, 0, 2)
    places = jnp.arange(span_len)
    lower = places[:, None] >= places[None, :]

    @jax.checkpoint
    def advance(carry, items):
        block_logs, block_inputs = items
        running = jnp.cumsum(block_logs, axis=1)
        spread = running[:, :, None] - running[:, None, :]
        weights = jnp.exp(jnp.where(lower[None], spread, far_below))
        inner = jnp.einsum("cts,cs->ct", weights, block_inputs, precision=highest)
        states = inner + jnp.exp(running) * carry[:, None]
        return (states[:, -1], states)

    start = jnp.zeros((channels,), jnp.float32)
    _, blocks = lax.scan(advance, start, (logs, inputs))
    return blocks.transpose(1, 0, 2).reshape(channels, length)


def mixer(branch, gate, shift, conv_weight, recur_weight, input_weight, decay_param):
    channels, length = branch.shape
    padded = jnp.pad(branch, ((0, 0), (CONV - 1, 0)))
    convolved = conv_weight[0][:, None] * padded[:, 0:length]
    for offset in range(1, CONV):
        convolved = convolved + conv_weight[offset][:, None] * padded[:, offset : offset + length]
    groups = channels // BLOCK_W
    grouped = convolved.reshape(groups, BLOCK_W, length)
    recur_gate = jax.nn.sigmoid(
        jnp.einsum("gil,gij->gjl", grouped, recur_weight, precision=highest).reshape(
            channels, length
        )
    )
    input_gate = jax.nn.sigmoid(
        jnp.einsum("gil,gij->gjl", grouped, input_weight, precision=highest).reshape(
            channels, length
        )
    )
    log_decay = -gate_const * recur_gate * jax.nn.softplus(-decay_param)[:, None] + jnp.repeat(
        shift, BLOCK_W, axis=0
    )
    pushed = jnp.sqrt(-jnp.expm1(2.0 * log_decay)) * input_gate * convolved
    states = block_states(log_decay, pushed)
    return states * jax.nn.gelu(gate)


def mixer_grads(
    branch, gate, shift, upstream, conv_weight, recur_weight, input_weight, decay_param
):

    def local(branch_f, gate_f, conv_f, recur_f, input_f, decay_f):
        return mixer(branch_f, gate_f, shift, conv_f, recur_f, input_f, decay_f)

    _, pullback = jax.vjp(
        local,
        branch.astype(jnp.float32),
        gate.astype(jnp.float32),
        conv_weight,
        recur_weight,
        input_weight,
        decay_param,
    )
    return pullback(upstream.astype(jnp.float32))


def body(
    normed,
    branch_in,
    gate_pre,
    cotangent,
    decay_shift,
    conv_weight,
    recur_weight,
    input_weight,
    decay_param,
    branch_proj,
):
    heads_cot = lax.all_to_all(cotangent, "sp", split_axis=1, concat_axis=2, tiled=True)
    grad_branch, grad_gate, grad_conv, grad_recur, grad_input, grad_decay = mixer_grads(
        branch_in[0],
        gate_pre[0],
        decay_shift[0],
        heads_cot[0],
        conv_weight,
        recur_weight,
        input_weight,
        decay_param,
    )
    small_sums = (
        lax.psum(grad_conv.astype(jnp.bfloat16), "dp").astype(jnp.float32),
        lax.psum(grad_recur.astype(jnp.bfloat16), "dp").astype(jnp.float32),
        lax.psum(grad_input.astype(jnp.bfloat16), "dp").astype(jnp.float32),
        lax.psum(grad_decay.astype(jnp.bfloat16), "dp").astype(jnp.float32),
    )
    branch_rounded = grad_branch.astype(jnp.bfloat16)[None]
    token_grad = lax.all_to_all(branch_rounded, "sp", split_axis=2, concat_axis=1, tiled=True)[0]
    grad_normed = jnp.dot(
        lax.all_gather(branch_proj, "dp", axis=0, tiled=True),
        token_grad,
        preferred_element_type=jnp.float32,
    ).astype(jnp.bfloat16)[None]
    partial_sum = lax.dot_general(
        normed[0], token_grad, (((1,), (1,)), ((), ())), preferred_element_type=jnp.float32
    )
    received = lax.all_to_all(
        partial_sum[None].astype(jnp.bfloat16), "dp", split_axis=1, concat_axis=0, tiled=True
    ).astype(jnp.float32)
    row_block = jnp.sum(received, axis=0)
    seq_count = lax.axis_size("sp")
    rows_here = row_block.shape[0]
    width_share = row_block.shape[1] // seq_count
    stacked = (
        row_block.reshape(rows_here, seq_count, width_share)
        .transpose(1, 0, 2)
        .reshape(seq_count * rows_here, width_share)
    )
    grad_proj = lax.psum_scatter(stacked, "sp", scatter_dimension=0, tiled=True)
    return (
        grad_normed,
        grad_gate.astype(jnp.bfloat16)[None],
        grad_proj,
        small_sums[0],
        small_sums[1],
        small_sums[2],
        small_sums[3],
    )


def solution(mesh):
    return jax.shard_map(
        body,
        mesh=mesh,
        in_specs=(
            P("dp", None, "sp"),
            P("dp", "sp", None),
            P("dp", "sp", None),
            P("dp", None, "sp"),
            P("dp", "sp", None),
            P(None, "sp"),
            P("sp", None, None),
            P("sp", None, None),
            P("sp"),
            P("dp", None),
        ),
        out_specs=(
            P("dp", None, "sp"),
            P("dp", "sp", None),
            P("dp", "sp"),
            P(None, "sp"),
            P("sp", None, None),
            P("sp", None, None),
            P("sp"),
        ),
        check_vma=False,
    )
```

profile of v0, /device:TPU:0, one launch (start us, length us, event | category | flops | bytes accessed | tf_op | source)
XLA Modules:
  0.0 484.7 jit_solution(2969427192037989468)
XLA Ops:
  8.0 1.4 copy.271
  10.0 2.2 reduce.1
  12.9 6.3 %all-to-all-start = ((bf16[4,2,16384]{2,1,0:T(2,128)(2,1)}), bf16[4,2,16384]{2,1,0:T(2,128)(2,1)}, u32[]{:S(2)}, u32[]{:S(2)}) async-start(bf16[4,2,16384]{2,1,0:T(2,128)(2,1)} %reshape.215), calls=%async_computation | async-start | bytes 524288 | tf_op jit(solution)/shard_map/all_to_all | solution.py:95
  19.3 1.3 broadcast_multiply_fusion.4
  28.3 1.3 add_bitcast_fusion.1
  30.4 131.4 %while.35 = (s32[]{:T(128)}, f32[256]{0:T(256)S(1)}, f32[4,256,128]{1,2,0:T(8,128)}, f32[4,256]{1,0:T(4,128)}, f32[4,256,128]{1,2,0:T(8,128)S(1)}, /*index=5*/f3...) while((s32[]{:T(128)}, f32[256]{0:T(256)S(1)}, ...), condition=%wide.region_2.3_spmd.clone, body=%wide.region_0.2_spmd.clone.sunk | while | flops 62947328 | bytes 2249857 | solution.py:34
  30.7 1.3 dynamic_update_slice.42
  32.3 27.3 %fusion.93 = f32[256,1,128]{2,1,0:T(1,128)S(1)} fusion(f32[256,128,1]{1,2,0:T(1,128)S(1)} %bitcast.252, f32[256,128]{1,0:T(8,128)S(1)} %copy.280, pred[128,128]{1,0:T(8,128)(4,1)S(1)} %get-tuple-element.650), kind=kOutput, calls=%fused_computation.2.clone.1 | convolution fusion | flops 58720256 | bytes 409600 | tf_op jit(solution)/shard_map/jvp()/while/body/eval_jaxpr/cts,cs->ct/dot_general | solution.py:29
  60.4 1.3 dynamic_update_slice.42
  62.0 27.3 %fusion.93 = f32[256,1,128]{2,1,0:T(1,128)S(1)} fusion(f32[256,128,1]{1,2,0:T(1,128)S(1)} %bitcast.252, f32[256,128]{1,0:T(8,128)S(1)} %copy.280, pred[128,128]{1,0:T(8,128)(4,1)S(1)} %get-tuple-element.650), kind=kOutput, calls=%fused_computation.2.clone.1 | convolution fusion | flops 58720256 | bytes 409600 | tf_op jit(solution)/shard_map/jvp()/while/body/eval_jaxpr/cts,cs->ct/dot_general | solution.py:29
  90.1 1.3 dynamic_update_slice.42
  91.7 27.3 %fusion.93 = f32[256,1,128]{2,1,0:T(1,128)S(1)} fusion(f32[256,128,1]{1,2,0:T(1,128)S(1)} %bitcast.252, f32[256,128]{1,0:T(8,128)S(1)} %copy.280, pred[128,128]{1,0:T(8,128)(4,1)S(1)} %get-tuple-element.650), kind=kOutput, calls=%fused_computation.2.clone.1 | convolution fusion | flops 58720256 | bytes 409600 | tf_op jit(solution)/shard_map/jvp()/while/body/eval_jaxpr/cts,cs->ct/dot_general | solution.py:29
  119.8 1.3 dynamic_update_slice.42
  121.4 27.3 %fusion.93 = f32[256,1,128]{2,1,0:T(1,128)S(1)} fusion(f32[256,128,1]{1,2,0:T(1,128)S(1)} %bitcast.252, f32[256,128]{1,0:T(8,128)S(1)} %copy.280, pred[128,128]{1,0:T(8,128)(4,1)S(1)} %get-tuple-element.650), kind=kOutput, calls=%fused_computation.2.clone.1 | convolution fusion | flops 58720256 | bytes 409600 | tf_op jit(solution)/shard_map/jvp()/while/body/eval_jaxpr/cts,cs->ct/dot_general | solution.py:29
  162.5 1.1 copy.222
  164.6 1.9 reshape.216
  168.2 2.0 fusion.29
  172.6 173.6 %while.36 = (s32[]{:T(128)}, f32[256]{0:T(256)}, f32[4,256,128]{1,2,0:T(8,128)}, f32[4,256,128]{2,1,0:T(8,128)}, f32[4,256]{1,0:T(4,128)}, /*index=5*/f32[4,256,...) while((s32[]{:T(128)}, f32[256]{0:T(256)}, ...), condition=%wide.region_9.10_spmd.clone, body=%wide.region_3.9_spmd.clone.sunk | while | flops 96616192 | bytes 5561497 | solution.py:34
  172.6 1.3 constant_dynamic-slice_fusion.7
  176.6 16.0 %fusion.96 = f32[256,1,128]{2,1,0:T(1,128)} fusion(f32[256,128,1]{1,2,0:T(1,128)S(1)} %copy.287, f32[256,128]{1,0:T(8,128)S(1)} %copy.283, pred[128,128]{1,0:T(8,128)(4,1)S(1)} %iota_compare_fusion.3), kind=kOutput, calls=%fused_computation.17.clone.1 | convolution fusion | flops 58720256 | bytes 409600 | tf_op jit(solution)/shard_map/transpose(jvp())/while/body/eval_jaxpr/checkpoint/cts,cs->ct/dot_general | solution.py:29
  193.3 16.3 %fusion.95 = (f32[256,128]{1,0:T(8,128)}, f32[256,128]{1,0:T(8,128)S(1)}) fusion(f32[256,128]{1,0:T(8,128)S(1)} %copy.283, f32[256,128]{1,0:T(8,128)S(1)} %dynamic-slice_bitcast_fusion.8, f32[256,128]{1,0:T(8,128)} %copy.284, pred[128,128]{1,0:T(8,128)(4,1)S(1)} %iota_compare_fusion.3), kind=kLoop, calls=%fused_computation.19.clone.1 | loop fusion | flops 29294592 | bytes 671744 | tf_op jit(solution)/shard_map/transpose(jvp())/while/body/eval_jaxpr/checkpoint/reduce_sum | solution.py:27
  211.5 2.2 reduce_window_sum.48
  214.3 1.6 bitcast_dynamic-update-slice_fusion.5
  215.9 1.3 constant_dynamic-slice_fusion.7
  220.0 16.0 %fusion.96 = f32[256,1,128]{2,1,0:T(1,128)} fusion(f32[256,128,1]{1,2,0:T(1,128)S(1)} %copy.287, f32[256,128]{1,0:T(8,128)S(1)} %copy.283, pred[128,128]{1,0:T(8,128)(4,1)S(1)} %iota_compare_fusion.3), kind=kOutput, calls=%fused_computation.17.clone.1 | convolution fusion | flops 58720256 | bytes 409600 | tf_op jit(solution)/shard_map/transpose(jvp())/while/body/eval_jaxpr/checkpoint/cts,cs->ct/dot_general | solution.py:29
  236.7 16.3 %fusion.95 = (f32[256,128]{1,0:T(8,128)}, f32[256,128]{1,0:T(8,128)S(1)}) fusion(f32[256,128]{1,0:T(8,128)S(1)} %copy.283, f32[256,128]{1,0:T(8,128)S(1)} %dynamic-slice_bitcast_fusion.8, f32[256,128]{1,0:T(8,128)} %copy.284, pred[128,128]{1,0:T(8,128)(4,1)S(1)} %iota_compare_fusion.3), kind=kLoop, calls=%fused_computation.19.clone.1 | loop fusion | flops 29294592 | bytes 671744 | tf_op jit(solution)/shard_map/transpose(jvp())/while/body/eval_jaxpr/checkpoint/reduce_sum | solution.py:27
  254.8 2.2 reduce_window_sum.48
  257.7 1.6 bitcast_dynamic-update-slice_fusion.5
  259.3 1.3 constant_dynamic-slice_fusion.7
  263.3 16.0 %fusion.96 = f32[256,1,128]{2,1,0:T(1,128)} fusion(f32[256,128,1]{1,2,0:T(1,128)S(1)} %copy.287, f32[256,128]{1,0:T(8,128)S(1)} %copy.283, pred[128,128]{1,0:T(8,128)(4,1)S(1)} %iota_compare_fusion.3), kind=kOutput, calls=%fused_computation.17.clone.1 | convolution fusion | flops 58720256 | bytes 409600 | tf_op jit(solution)/shard_map/transpose(jvp())/while/body/eval_jaxpr/checkpoint/cts,cs->ct/dot_general | solution.py:29
  280.0 16.3 %fusion.95 = (f32[256,128]{1,0:T(8,128)}, f32[256,128]{1,0:T(8,128)S(1)}) fusion(f32[256,128]{1,0:T(8,128)S(1)} %copy.283, f32[256,128]{1,0:T(8,128)S(1)} %dynamic-slice_bitcast_fusion.8, f32[256,128]{1,0:T(8,128)} %copy.284, pred[128,128]{1,0:T(8,128)(4,1)S(1)} %iota_compare_fusion.3), kind=kLoop, calls=%fused_computation.19.clone.1 | loop fusion | flops 29294592 | bytes 671744 | tf_op jit(solution)/shard_map/transpose(jvp())/while/body/eval_jaxpr/checkpoint/reduce_sum | solution.py:27
  298.2 2.2 reduce_window_sum.48
  301.0 1.6 bitcast_dynamic-update-slice_fusion.5
  302.6 1.3 constant_dynamic-slice_fusion.7
  306.6 16.0 %fusion.96 = f32[256,1,128]{2,1,0:T(1,128)} fusion(f32[256,128,1]{1,2,0:T(1,128)S(1)} %copy.287, f32[256,128]{1,0:T(8,128)S(1)} %copy.283, pred[128,128]{1,0:T(8,128)(4,1)S(1)} %iota_compare_fusion.3), kind=kOutput, calls=%fused_computation.17.clone.1 | convolution fusion | flops 58720256 | bytes 409600 | tf_op jit(solution)/shard_map/transpose(jvp())/while/body/eval_jaxpr/checkpoint/cts,cs->ct/dot_general | solution.py:29
  323.4 16.3 %fusion.95 = (f32[256,128]{1,0:T(8,128)}, f32[256,128]{1,0:T(8,128)S(1)}) fusion(f32[256,128]{1,0:T(8,128)S(1)} %copy.283, f32[256,128]{1,0:T(8,128)S(1)} %dynamic-slice_bitcast_fusion.8, f32[256,128]{1,0:T(8,128)} %copy.284, pred[128,128]{1,0:T(8,128)(4,1)S(1)} %iota_compare_fusion.3), kind=kLoop, calls=%fused_computation.19.clone.1 | loop fusion | flops 29294592 | bytes 671744 | tf_op jit(solution)/shard_map/transpose(jvp())/while/body/eval_jaxpr/checkpoint/reduce_sum | solution.py:27
  341.5 2.2 reduce_window_sum.48
  344.4 1.6 bitcast_dynamic-update-slice_fusion.5
  346.2 2.1 copy.250
  348.3 2.1 copy.231
  350.4 1.2 copy.232
  351.7 2.9 fusion.52
  354.5 1.3 convolution_convert_fusion.1
  355.8 1.4 fusion.67
  357.2 1.2 copy.241
  358.3 2.1 reshape.202
  360.9 1.2 fusion.45
  362.2 1.3 convolution_convert_fusion.2
  363.4 2.3 fusion.48
  369.3 2.2 reduce.2
  371.6 13.2 %all_to_all.33 = bf16[4,2,16384]{2,1,0:T(2,128)(2,1)S(1)} all-to-all(bf16[4,2,16384]{2,1,0:T(2,128)(2,1)S(1)} %reshape.217), channel_id=1, replica_groups=mesh['sp'=4,'dp'=8] {'sp'}, dimensions={0} | all-to-all | bytes 524288 | tf_op jit(solution)/shard_map/all_to_all | solution.py:113
  386.0 7.7 %copy.238 = bf16[1,1024,1024]{2,0,1:T(2,128)(2,1)} copy(bf16[1,1024,1024]{1,2,0:T(8,128)(2,1)S(1)} %convert_bitcast_fusion) | data formatting | bytes 4194304 | tf_op jit(solution)/shard_map/convert_element_type | solution.py:123
  393.8 12.7 %reduce.3 = bf16[1024,1024]{1,0:T(8,128)(2,1)S(1)} reduce(bf16[1024,1,1024]{2,1,0:T(2,128)(2,1)} %bitcast.238, bf16[]{:T(256)} %broadcast.172), dimensions={1}, to_apply=%bitcast.175.reduce_sub_computation | reduce | bytes 4194306
  406.5 3.8 reshape.219
  410.3 33.4 %all_to_all.34 = bf16[8,2,65536]{2,1,0:T(2,128)(2,1)S(1)} all-to-all(bf16[8,2,65536]{2,1,0:T(2,128)(2,1)} %reshape.219), channel_id=1, replica_groups=mesh['sp'=4,'dp'=8] {'dp'}, dimensions={0} | all-to-all | bytes 4194304 | tf_op jit(solution)/shard_map/all_to_all | solution.py:122
  443.7 4.4 reshape.220
  448.1 5.2 %copy.254 = f32[1,1024,1024]{2,1,0:T(8,128)} copy(bf16[1,1024,1024]{2,0,1:T(2,128)(2,1)} %bitcast.240) | data formatting | bytes 6291456
  453.3 2.7 reduce_sum.117
  458.7 1.2 convert_element_type.132
  459.9 1.3 convert_element_type.126
  461.2 1.5 convert_element_type.128
  462.7 1.5 convert_element_type.130
  464.2 2.4 fusion.27
  467.4 9.4 %reduce-scatter.2.cloned.1.call-done = f32[128,256]{1,0:T(8,128)} async-done(((f32[512,256]{1,0:T(8,128)}), f32[128,256]{1,0:T(8,128)}) %reduce-scatter.2.cloned.1.call-update) | async-done | bytes 131088 | tf_op jit(solution)/shard_map/reduce_scatter | solution.py:134
  (195 shorter events, 52.5 us)
Async XLA Ops:
  8.0 377.3 %copy-start = (bf16[1,1024,128]{2,1,0:T(8,128)(2,1)S(1)}, bf16[1,1024,128]{2,1,0:T(8,128)(2,1)}, u32[]{:S(2)}) copy-start(bf16[1,1024,128]{2,1,0:T(8,128)(2,1)} %param.14) | copy-start | bytes 786436
  8.0 15.1 %copy-start.13 = (f32[4,64,64]{2,1,0:T(8,128)S(1)}, f32[4,64,64]{2,1,0:T(8,128)}, u32[]{:S(2)}) copy-start(f32[4,64,64]{2,1,0:T(8,128)} %param.20) | copy-start | bytes 196612
  8.0 15.9 %copy-start.11 = (f32[4,64,64]{2,1,0:T(8,128)S(1)}, f32[4,64,64]{2,1,0:T(8,128)}, u32[]{:S(2)}) copy-start(f32[4,64,64]{2,1,0:T(8,128)} %param.21) | copy-start | bytes 196612
  9.4 15.2 %copy-start.9 = (f32[1,4,512]{2,1,0:T(4,128)S(1)}, f32[1,4,512]{2,1,0:T(4,128)}, u32[]{:S(2)}) copy-start(f32[1,4,512]{2,1,0:T(4,128)} %param.18) | copy-start | bytes 24580
  12.9 151.6 %all-to-all-start = ((bf16[4,2,16384]{2,1,0:T(2,128)(2,1)}), bf16[4,2,16384]{2,1,0:T(2,128)(2,1)}, u32[]{:S(2)}, u32[]{:S(2)}) async-start(bf16[4,2,16384]{2,1,0:T(2,128)(2,1)} %reshape.215), calls=%async_computation | async-start | bytes 524288 | tf_op jit(solution)/shard_map/all_to_all | solution.py:95
  19.3 439.4 %all-reduce.13.cloned.1.call-start = ((), (), s32[]{:S(2)}) async-start(), calls=%async_computation.6 | async-start | bytes 267264 | tf_op jit(solution)/shard_map/psum | solution.py:107
  20.6 141.3 %copy-start.14 = (f32[256]{0:T(256)}, f32[256]{0:T(256)S(1)}, u32[]{:S(2)}) copy-start(f32[256]{0:T(256)S(1)} %get-tuple-element.495) | copy-start | bytes 3076
  21.4 4.1 copy-start.16
  21.4 4.1 copy-start.18
  21.4 4.1 copy-start.20
  21.4 4.1 copy-start.22
  23.1 0.8 copy-start.1
  163.6 8.9 %copy-start.6 = (bf16[1,256,512]{1,2,0:T(8,128)(2,1)}, bf16[1,256,512]{1,2,0:T(8,128)(2,1)S(1)}, u32[]{:S(2)}) copy-start(bf16[1,256,512]{1,2,0:T(8,128)(2,1)S(1)} %copy.222) | copy-start | bytes 786436
  167.5 0.7 copy-start.4
  346.1 8.4 %copy-start.2 = (f32[256,512]{1,0:T(8,128)S(1)}, f32[256,512]{1,0:T(8,128)}, u32[]{:S(2)}) copy-start(f32[256,512]{1,0:T(8,128)} %copy-done.1) | copy-start | bytes 1572868
  348.3 8.9 %copy-start.3 = (f32[4,256,128]{2,1,0:T(8,128)S(1)}, f32[4,256,128]{2,1,0:T(8,128)}, u32[]{:S(2)}) copy-start(f32[4,256,128]{2,1,0:T(8,128)} %get-tuple-element.258) | copy-start | bytes 1572868
  351.6 4.2 copy-start.12
  351.6 8.8 %copy-start.24 = (f32[256]{0:T(256)S(1)}, f32[256]{0:T(256)}, u32[]{:S(2)}) copy-start(f32[256]{0:T(256)} %get-tuple-element.496) | copy-start | bytes 3076
  351.7 8.7 %copy-start.26 = (f32[256]{0:T(256)S(1)}, f32[256]{0:T(256)}, u32[]{:S(2)}) copy-start(f32[256]{0:T(256)} %param.22) | copy-start | bytes 3076
  354.5 8.9 %copy-start.10 = (f32[1,4,512]{2,1,0:T(4,128)S(1)}, f32[1,4,512]{2,1,0:T(4,128)}, u32[]{:S(2)}) copy-start(f32[1,4,512]{2,1,0:T(4,128)} %param.18) | copy-start | bytes 24580
  354.5 8.9 %copy-start.25 = (f32[4,64]{1,0:T(4,128)S(1)}, f32[4,64]{1,0:T(4,128)}, u32[]{:S(2)}) copy-start(f32[4,64]{1,0:T(4,128)} %mul.371) | copy-start | bytes 3076
  357.2 8.6 %copy-start.15 = (f32[256]{0:T(256)S(1)}, f32[256]{0:T(256)}, u32[]{:S(2)}) copy-start(f32[256]{0:T(256)} %copy-done.14) | copy-start | bytes 3076
  362.1 6.0 %copy-start.17 = (f32[1,256]{1,0:T(1,128)S(1)}, f32[1,256]{1,0:T(1,128)}, u32[]{:S(2)}) copy-start(f32[1,256]{1,0:T(1,128)} %copy-done.16) | copy-start | bytes 3076
  362.1 6.0 %copy-start.19 = (f32[1,256]{1,0:T(1,128)S(1)}, f32[1,256]{1,0:T(1,128)}, u32[]{:S(2)}) copy-start(f32[1,256]{1,0:T(1,128)} %copy-done.18) | copy-start | bytes 3076
  362.2 6.0 %copy-start.21 = (f32[1,256]{1,0:T(1,128)S(1)}, f32[1,256]{1,0:T(1,128)}, u32[]{:S(2)}) copy-start(f32[1,256]{1,0:T(1,128)} %copy-done.20) | copy-start | bytes 3076
  362.2 6.0 %copy-start.23 = (f32[1,256]{1,0:T(1,128)S(1)}, f32[1,256]{1,0:T(1,128)}, u32[]{:S(2)}) copy-start(f32[1,256]{1,0:T(1,128)} %copy-done.22) | copy-start | bytes 3076
  367.4 96.8 %all-gather.2.cloned.1.call-start = ((), (), s32[]{:S(2)}) async-start(), calls=%async_computation.4 | async-start | bytes 2359296 | tf_op jit(solution)/shard_map/all_gather | solution.py:115
  368.1 108.8 %reduce-scatter.2.cloned.1.call-start = ((), (), s32[]{:S(2)}) async-start(), calls=%async_computation.5 | async-start | bytes 655360 | tf_op jit(solution)/shard_map/reduce_scatter | solution.py:134
  453.3 4.0 copy-start.5
  453.3 4.2 copy-start.7
  453.3 4.2 copy-start.8
Sparse Core Ops, SparseCore 0:
  367.5 53.7 all-reduce.12
  423.2 32.6 all-gather.1
Sparse Core Ops, SparseCore 1:
  457.3 19.5 reduce-scatter.1
where the time goes:
time: 492 us; the launch traced here: 485 us
  matrix products  184 us (37%)
  other arithmetic  123 us (25%)
  local copies, waits for them, and re-layouts  85.1 us (17%)
  blocking collectives  46.6 us (9%)
  between operations  16.5 us (3%)
  loops' own time  13.2 us (3%)
  waiting for transfers between devices  10.1 us (2%)
  starting transfers between devices  6.43 us (1%)
    dot_general x8, matrix products, advance(): inner = jnp.einsum('cts,cs->ct', weights, block_inputs, precision=highest)  173 us
    reduce_sum x4, other arithmetic, advance(): spread = running[:, :, None] - running[:, None, :]  65.3 us
    all_to_all x1, blocking collectives, body(): lax.all_to_all(partial_sum[None].astype(jnp.bfloat16), 'dp', split_axis=1...  33.4 us
    unnamed x68, local copies, waits for them, and re-layouts  22.2 us
    unnamed x3, other arithmetic  17.1 us
    dynamic_update_slice x12, local copies, waits for them, and re-layouts, block_states(): _, blocks = lax.scan(advance, start, (logs, inputs))  14.2 us
    another operation x2, loops' own time, block_states(): _, blocks = lax.scan(advance, start, (logs, inputs))  13.2 us
    all_to_all x1, blocking collectives, body(): lax.all_to_all(branch_rounded, 'sp', split_axis=2, concat_axis=1, tiled=T...  13.2 us
  transfers between devices with their start and end apart: 4, of which 1 were waited for; matrix products, arithmetic and copies ran while one was open for 38% of the time, Pallas kernels for 0%

commit v1 on v0

--- a/solution.py
+++ b/solution.py
@@ -119,8 +119,16 @@
     partial_sum = lax.dot_general(
         normed[0], token_grad, (((1,), (1,)), ((), ())), preferred_element_type=jnp.float32
     )
-    received = lax.all_to_all(
-        partial_sum[None].astype(jnp.bfloat16), "dp", split_axis=1, concat_axis=0, tiled=True
+    received = jnp.concatenate(
+        lax.all_to_all(
+            jnp.stack(
+                jnp.split(partial_sum[None].astype(jnp.bfloat16), lax.axis_size("dp"), axis=1)
+            ),
+            "dp",
+            0,
+            0,
+        ),
+        axis=0,
     ).astype(jnp.float32)
     row_block = jnp.sum(received, axis=0)
     seq_count = lax.axis_size("sp")

time: 492 us -> 467 us (0.949)
  waiting for transfers between devices: 10.1 us -> 46.9 us
  local copies, waits for them, and re-layouts: 85.1 us -> 55.4 us
  other arithmetic: 123 us -> 106 us
  blocking collectives: 46.6 us -> 30.7 us
  starting transfers between devices: 6.43 us -> 11.5 us
    all_gather x1, waiting for transfers between devices: 0.01 us -> 25 us  [body(): lax.all_gather(branch_proj, 'dp', axis=0, tiled=True)]
    all_to_all x2 -> x1, blocking collectives: 46.6 us -> 30.7 us  [body(): lax.all_to_all(jnp.stack(jnp.split(partial_sum[None].astype(jnp.bfloat16)...]
    psum x1, waiting for transfers between devices: 0.01 us -> 15.5 us  [body(): lax.psum(grad_conv.astype(jnp.bfloat16), 'dp').astype(jnp.float32)]
    unnamed x3 -> x2, other arithmetic: 17.1 us -> 4.36 us
    unnamed x68 -> x100, local copies, waits for them, and re-layouts: 22.2 us -> 10.1 us
    reduce_scatter x1, waiting for transfers between devices: 9.41 us -> 0.01 us  [body(): grad_proj = lax.psum_scatter(stacked, 'sp', scatter_dimension=0, tiled=True)]
    convert_element_type x1 -> x0, local copies, waits for them, and re-layouts: 7.74 us -> none  [body(): partial_sum[None].astype(jnp.bfloat16)]
    all_to_all x0 -> x1, waiting for transfers between devices: none -> 5.65 us  [body(): lax.all_to_all(branch_rounded, 'sp', split_axis=2, concat_axis=1, tiled=T...]
  transfers between devices with their start and end apart: 4 -> 5, of which waited for: 1 -> 3; matrix products, arithmetic and copies ran while one was open for 38% -> 31% of each run, Pallas kernels for 0% -> 0%
where the time goes in v1:
time: 467 us; the launch traced here: 460 us
  matrix products  180 us (39%)
  other arithmetic  106 us (23%)
  local copies, waits for them, and re-layouts  55.4 us (12%)
  waiting for transfers between devices  46.9 us (10%)
  blocking collectives  30.7 us (7%)
  between operations  16.6 us (4%)
  loops' own time  13.2 us (3%)
  starting transfers between devices  11.5 us (2%)
    dot_general x8, matrix products, advance(): inner = jnp.einsum('cts,cs->ct', weights, block_inputs, precision=highest)  170 us
    reduce_sum x4, other arithmetic, advance(): spread = running[:, :, None] - running[:, None, :]  65.3 us
    all_to_all x1, blocking collectives, body(): lax.all_to_all(jnp.stack(jnp.split(partial_sum[None].astype(jnp.bfloat16)...  30.7 us
    all_gather x1, waiting for transfers between devices, body(): lax.all_gather(branch_proj, 'dp', axis=0, tiled=True)  25 us
    psum x1, waiting for transfers between devices, body(): lax.psum(grad_conv.astype(jnp.bfloat16), 'dp').astype(jnp.float32)  15.5 us
    another operation x16, other arithmetic, advance(): running = jnp.cumsum(block_logs, axis=1)  13.2 us
    another operation x2, loops' own time, block_states(): _, blocks = lax.scan(advance, start, (logs, inputs))  13.2 us
    dynamic_update_slice x12, local copies, waits for them, and re-layouts, block_states(): _, blocks = lax.scan(advance, start, (logs, inputs))  10.5 us
  transfers between devices with their start and end apart: 5, of which 3 were waited for; matrix products, arithmetic and copies ran while one was open for 31% of the time, Pallas kernels for 0%

profile of v1, /device:TPU:0, one launch (start us, length us, event | category | flops | bytes accessed | tf_op | source)
XLA Modules:
  0.0 460.2 jit_solution(629386554679617187)
XLA Ops:
  8.0 1.4 copy.231
  10.0 2.2 reduce.2
  13.0 6.3 %all-to-all-start = ((bf16[4,2,16384]{2,1,0:T(2,128)(2,1)}), bf16[4,2,16384]{2,1,0:T(2,128)(2,1)}, u32[]{:S(2)}, u32[]{:S(2)}) async-start(bf16[4,2,16384]{2,1,0:T(2,128)(2,1)} %reshape.211), calls=%async_computation | async-start | bytes 524288 | tf_op jit(solution)/shard_map/all_to_all | solution.py:95
  23.5 1.0 copy.179
  25.0 1.1 add_bitcast_fusion.1
  27.0 131.4 %while.35 = (s32[]{:T(128)}, f32[256]{0:T(256)S(1)}, f32[4,256,128]{1,2,0:T(8,128)}, f32[4,256]{1,0:T(4,128)}, f32[4,256,128]{1,2,0:T(8,128)S(1)}, /*index=5*/f3...) while((s32[]{:T(128)}, f32[256]{0:T(256)S(1)}, ...), condition=%wide.region_2.3_spmd.clone, body=%wide.region_0.2_spmd.clone.sunk | while | flops 62947328 | bytes 2250357 | solution.py:34
  27.5 27.3 %fusion.101 = f32[256,1,128]{2,1,0:T(1,128)S(1)} fusion(f32[256,128,1]{1,2,0:T(1,128)S(1)} %bitcast.277, f32[256,128]{1,0:T(8,128)S(1)} %copy.240, pred[128,128]{1,0:T(8,128)(4,1)S(1)} %get-tuple-element.628), kind=kOutput, calls=%fused_computation.2.clone.1 | convolution fusion | flops 58720256 | bytes 409600 | tf_op jit(solution)/shard_map/jvp()/while/body/eval_jaxpr/cts,cs->ct/dot_general | solution.py:29
  55.6 1.3 dynamic_update_slice.42
  57.2 27.3 %fusion.101 = f32[256,1,128]{2,1,0:T(1,128)S(1)} fusion(f32[256,128,1]{1,2,0:T(1,128)S(1)} %bitcast.277, f32[256,128]{1,0:T(8,128)S(1)} %copy.240, pred[128,128]{1,0:T(8,128)(4,1)S(1)} %get-tuple-element.628), kind=kOutput, calls=%fused_computation.2.clone.1 | convolution fusion | flops 58720256 | bytes 409600 | tf_op jit(solution)/shard_map/jvp()/while/body/eval_jaxpr/cts,cs->ct/dot_general | solution.py:29
  85.3 1.3 dynamic_update_slice.42
  86.9 27.3 %fusion.101 = f32[256,1,128]{2,1,0:T(1,128)S(1)} fusion(f32[256,128,1]{1,2,0:T(1,128)S(1)} %bitcast.277, f32[256,128]{1,0:T(8,128)S(1)} %copy.240, pred[128,128]{1,0:T(8,128)(4,1)S(1)} %get-tuple-element.628), kind=kOutput, calls=%fused_computation.2.clone.1 | convolution fusion | flops 58720256 | bytes 409600 | tf_op jit(solution)/shard_map/jvp()/while/body/eval_jaxpr/cts,cs->ct/dot_general | solution.py:29
  115.0 1.3 dynamic_update_slice.42
  116.6 27.3 %fusion.101 = f32[256,1,128]{2,1,0:T(1,128)S(1)} fusion(f32[256,128,1]{1,2,0:T(1,128)S(1)} %bitcast.277, f32[256,128]{1,0:T(8,128)S(1)} %copy.240, pred[128,128]{1,0:T(8,128)(4,1)S(1)} %get-tuple-element.628), kind=kOutput, calls=%fused_computation.2.clone.1 | convolution fusion | flops 58720256 | bytes 409600 | tf_op jit(solution)/shard_map/jvp()/while/body/eval_jaxpr/cts,cs->ct/dot_general | solution.py:29
  144.7 1.3 dynamic_update_slice.42
  159.0 1.1 copy.185
  160.1 0.9 copy.190
  161.1 1.9 reshape.212
  162.9 1.1 copy.184
  164.7 2.0 fusion.29
  169.1 167.3 %while.36 = (s32[]{:T(128)}, f32[256]{0:T(256)}, f32[4,256,128]{1,2,0:T(8,128)}, f32[4,256,128]{2,1,0:T(8,128)}, f32[4,256]{1,0:T(4,128)}, /*index=5*/f32[4,256,...) while((s32[]{:T(128)}, f32[256]{0:T(256)}, ...), condition=%wide.region_9.10_spmd.clone, body=%wide.region_3.9_spmd.clone.sunk | while | flops 96616192 | bytes 5561497 | solution.py:34
  169.1 0.9 constant_dynamic-slice_fusion.8
  170.1 1.3 constant_dynamic-slice_fusion.7
  173.1 15.3 %fusion.104 = f32[256,1,128]{2,1,0:T(1,128)S(1)} fusion(f32[256,128,1]{1,2,0:T(1,128)S(1)} %copy.247, f32[256,128]{1,0:T(8,128)S(1)} %copy.243, pred[128,128]{1,0:T(8,128)(4,1)S(1)} %iota_compare_fusion.3), kind=kOutput, calls=%fused_computation.17.clone.1 | convolution fusion | flops 58720256 | bytes 409600 | tf_op jit(solution)/shard_map/transpose(jvp())/while/body/eval_jaxpr/checkpoint/cts,cs->ct/dot_general | solution.py:29
  189.8 16.3 %fusion.103 = (f32[256,128]{1,0:T(8,128)}, f32[256,128]{1,0:T(8,128)S(1)}) fusion(f32[256,128]{1,0:T(8,128)S(1)} %copy.243, f32[256,128]{1,0:T(8,128)S(1)} %dynamic-slice_bitcast_fusion.8, f32[256,128]{1,0:T(8,128)} %copy.244, pred[128,128]{1,0:T(8,128)(4,1)S(1)} %iota_compare_fusion.3), kind=kLoop, calls=%fused_computation.19.clone.1 | loop fusion | flops 29294592 | bytes 671744 | tf_op jit(solution)/shard_map/transpose(jvp())/while/body/eval_jaxpr/checkpoint/reduce_sum | solution.py:27
  206.2 1.0 copy.246
  208.0 2.2 reduce_window_sum.48
  210.8 0.9 constant_dynamic-slice_fusion.8
  211.9 1.3 constant_dynamic-slice_fusion.7
  214.9 15.3 %fusion.104 = f32[256,1,128]{2,1,0:T(1,128)S(1)} fusion(f32[256,128,1]{1,2,0:T(1,128)S(1)} %copy.247, f32[256,128]{1,0:T(8,128)S(1)} %copy.243, pred[128,128]{1,0:T(8,128)(4,1)S(1)} %iota_compare_fusion.3), kind=kOutput, calls=%fused_computation.17.clone.1 | convolution fusion | flops 58720256 | bytes 409600 | tf_op jit(solution)/shard_map/transpose(jvp())/while/body/eval_jaxpr/checkpoint/cts,cs->ct/dot_general | solution.py:29
  231.6 16.3 %fusion.103 = (f32[256,128]{1,0:T(8,128)}, f32[256,128]{1,0:T(8,128)S(1)}) fusion(f32[256,128]{1,0:T(8,128)S(1)} %copy.243, f32[256,128]{1,0:T(8,128)S(1)} %dynamic-slice_bitcast_fusion.8, f32[256,128]{1,0:T(8,128)} %copy.244, pred[128,128]{1,0:T(8,128)(4,1)S(1)} %iota_compare_fusion.3), kind=kLoop, calls=%fused_computation.19.clone.1 | loop fusion | flops 29294592 | bytes 671744 | tf_op jit(solution)/shard_map/transpose(jvp())/while/body/eval_jaxpr/checkpoint/reduce_sum | solution.py:27
  248.0 1.0 copy.246
  249.7 2.2 reduce_window_sum.48
  253.7 1.3 constant_dynamic-slice_fusion.7
  256.6 15.3 %fusion.104 = f32[256,1,128]{2,1,0:T(1,128)S(1)} fusion(f32[256,128,1]{1,2,0:T(1,128)S(1)} %copy.247, f32[256,128]{1,0:T(8,128)S(1)} %copy.243, pred[128,128]{1,0:T(8,128)(4,1)S(1)} %iota_compare_fusion.3), kind=kOutput, calls=%fused_computation.17.clone.1 | convolution fusion | flops 58720256 | bytes 409600 | tf_op jit(solution)/shard_map/transpose(jvp())/while/body/eval_jaxpr/checkpoint/cts,cs->ct/dot_general | solution.py:29
  273.4 16.3 %fusion.103 = (f32[256,128]{1,0:T(8,128)}, f32[256,128]{1,0:T(8,128)S(1)}) fusion(f32[256,128]{1,0:T(8,128)S(1)} %copy.243, f32[256,128]{1,0:T(8,128)S(1)} %dynamic-slice_bitcast_fusion.8, f32[256,128]{1,0:T(8,128)} %copy.244, pred[128,128]{1,0:T(8,128)(4,1)S(1)} %iota_compare_fusion.3), kind=kLoop, calls=%fused_computation.19.clone.1 | loop fusion | flops 29294592 | bytes 671744 | tf_op jit(solution)/shard_map/transpose(jvp())/while/body/eval_jaxpr/checkpoint/reduce_sum | solution.py:27
  289.8 1.0 copy.246
  291.5 2.2 reduce_window_sum.48
  294.4 0.9 constant_dynamic-slice_fusion.8
  295.5 1.3 constant_dynamic-slice_fusion.7
  298.4 15.3 %fusion.104 = f32[256,1,128]{2,1,0:T(1,128)S(1)} fusion(f32[256,128,1]{1,2,0:T(1,128)S(1)} %copy.247, f32[256,128]{1,0:T(8,128)S(1)} %copy.243, pred[128,128]{1,0:T(8,128)(4,1)S(1)} %iota_compare_fusion.3), kind=kOutput, calls=%fused_computation.17.clone.1 | convolution fusion | flops 58720256 | bytes 409600 | tf_op jit(solution)/shard_map/transpose(jvp())/while/body/eval_jaxpr/checkpoint/cts,cs->ct/dot_general | solution.py:29
  315.1 16.3 %fusion.103 = (f32[256,128]{1,0:T(8,128)}, f32[256,128]{1,0:T(8,128)S(1)}) fusion(f32[256,128]{1,0:T(8,128)S(1)} %copy.243, f32[256,128]{1,0:T(8,128)S(1)} %dynamic-slice_bitcast_fusion.8, f32[256,128]{1,0:T(8,128)} %copy.244, pred[128,128]{1,0:T(8,128)(4,1)S(1)} %iota_compare_fusion.3), kind=kLoop, calls=%fused_computation.19.clone.1 | loop fusion | flops 29294592 | bytes 671744 | tf_op jit(solution)/shard_map/transpose(jvp())/while/body/eval_jaxpr/checkpoint/reduce_sum | solution.py:27
  331.5 1.0 copy.246
  333.3 2.2 reduce_window_sum.48
  336.4 1.3 copy.194
  338.2 2.3 fusion.52
  340.5 1.4 fusion.75
  341.9 1.4 copy.202
  343.4 1.0 reshape.199
  344.4 1.3 fusion.45
  345.7 1.3 convolution_convert_fusion.2
  347.0 1.6 fusion.48
  351.3 2.2 reduce.3
  354.3 5.1 %all-to-all-start.1 = ((bf16[4,2,16384]{2,1,0:T(2,128)(2,1)}), bf16[4,2,16384]{2,1,0:T(2,128)(2,1)S(1)}, u32[]{:S(2)}, u32[]{:S(2)}) async-start(bf16[4,2,16384]{2,1,0:T(2,128)(2,1)} %reshape.213), calls=%async_computation.1 | async-start | bytes 524288 | tf_op jit(solution)/shard_map/all_to_all | solution.py:113
  360.0 1.2 convolution_convert_fusion.1
  362.0 5.6 %all-to-all-done.1 = bf16[4,2,16384]{2,1,0:T(2,128)(2,1)S(1)} async-done(((bf16[4,2,16384]{2,1,0:T(2,128)(2,1)}), bf16[4,2,16384]{2,1,0:T(2,128)(2,1)S(1)}, u32[]{:S(2)}, u32[]{:S(2)}) %all-to-all-start.1) | async-done | bytes 262176 | tf_op jit(solution)/shard_map/all_to_all | solution.py:113
  369.6 30.7 %all_to_all.29 = bf16[8,1,128,1024]{2,3,1,0:T(8,128)(2,1)S(1)} all-to-all(bf16[8,1,128,1024]{2,3,1,0:T(8,128)(2,1)S(1)} %fusion.60), channel_id=1, replica_groups=mesh['sp'=4,'dp'=8] {'dp'}, dimensions={0} | all-to-all | bytes 4194304 | tf_op jit(solution)/shard_map/all_to_all | solution.py:123
  400.6 1.0 copy.201
  403.2 15.5 %all-reduce.13.cloned.1.call-done = (bf16[4,256]{1,0:T(4,128)(2,1)}, bf16[4,64,64]{2,1,0:T(8,128)(2,1)}, bf16[4,64,64]{2,1,0:T(8,128)(2,1)}, bf16[256]{0:T(256)(128)(2,1)}) async-done(((bf16[4,256]{1,0:T(4,128)(2,1)}, bf16[4,64,64]{2,1,0:T(8,128)(2,1)}, bf16[4,64,64]{2,1,0:T(8,128)(2,1)}, bf16[256]{0:T(256)(128)(2,1)}), (bf16[4,256]{1,0:T(4,128)(2,1)}, bf16[4,64,64]{2,1,0:T(8,128)(2,1)}, ...) | async-done | bytes 68112 | tf_op jit(solution)/shard_map/psum | solution.py:107
  418.7 1.5 convert_element_type.122
  420.2 1.5 convert_element_type.124
  421.7 1.3 convert_element_type.120
  422.9 1.1 convert_element_type.126
  424.1 25.0 %all-gather.2.cloned.1.call-done = bf16[1024,1024]{1,0:T(8,128)(2,1)} async-done(((bf16[128,1024]{1,0:T(8,128)(2,1)}), bf16[1024,1024]{1,0:T(8,128)(2,1)}) %all-gather.2.cloned.1.call-update) | async-done | bytes 2097168 | tf_op jit(solution)/shard_map/all_gather | solution.py:115
  449.1 2.4 fusion.27
  (226 shorter events, 44.1 us)
Async XLA Ops:
  8.0 360.2 %copy-start = (bf16[1,1024,128]{2,1,0:T(8,128)(2,1)S(1)}, bf16[1,1024,128]{2,1,0:T(8,128)(2,1)}, u32[]{:S(2)}) copy-start(bf16[1,1024,128]{2,1,0:T(8,128)(2,1)} %param.14) | copy-start | bytes 786436
  8.0 11.4 %copy-start.39 = (f32[4,256]{1,0:T(4,128)S(1)}, f32[4,256]{1,0:T(4,128)}, u32[]{:S(2)}) copy-start(f32[4,256]{1,0:T(4,128)} %param.19) | copy-start | bytes 12292
  8.0 11.4 %copy-start.13 = (bf16[1,256,512]{2,1,0:T(8,128)(2,1)S(1)}, bf16[1,256,512]{2,1,0:T(8,128)(2,1)}, u32[]{:S(2)}) copy-start(bf16[1,256,512]{2,1,0:T(8,128)(2,1)} %param.15) | copy-start | bytes 786436
  8.0 12.1 %copy-start.19 = (f32[4,64,64]{2,1,0:T(8,128)S(1)}, f32[4,64,64]{2,1,0:T(8,128)}, u32[]{:S(2)}) copy-start(f32[4,64,64]{2,1,0:T(8,128)} %param.20) | copy-start | bytes 196612
  13.0 148.1 %all-to-all-start = ((bf16[4,2,16384]{2,1,0:T(2,128)(2,1)}), bf16[4,2,16384]{2,1,0:T(2,128)(2,1)}, u32[]{:S(2)}, u32[]{:S(2)}) async-start(bf16[4,2,16384]{2,1,0:T(2,128)(2,1)} %reshape.211), calls=%async_computation | async-start | bytes 524288 | tf_op jit(solution)/shard_map/all_to_all | solution.py:95
  19.3 1.6 copy-start.17
  19.4 2.8 copy-start.23
  19.4 2.8 copy-start.25
  19.4 2.8 copy-start.28
  19.4 2.8 copy-start.31
  20.2 1.5 copy-start.1
  20.2 1.4 copy-start.37
  20.2 2.0 copy-start.15
  22.2 136.2 %copy-start.21 = (f32[256]{0:T(256)}, f32[256]{0:T(256)S(1)}, u32[]{:S(2)}) copy-start(f32[256]{0:T(256)S(1)} %get-tuple-element.473) | copy-start | bytes 3076
  160.1 7.5 %copy-start.7 = (bf16[1,256,512]{1,2,0:T(8,128)(2,1)}, bf16[1,256,512]{1,2,0:T(8,128)(2,1)S(1)}, u32[]{:S(2)}) copy-start(bf16[1,256,512]{1,2,0:T(8,128)(2,1)S(1)} %copy.185) | copy-start | bytes 786436
  164.0 0.7 copy-start.5
  336.4 1.6 copy-start.10
  336.4 1.8 copy-start.16
  336.4 1.8 copy-start.22
  336.4 1.8 copy-start.24
  336.4 1.8 copy-start.26
  336.4 1.8 copy-start.29
  336.4 1.8 copy-start.32
  337.9 2.6 copy-start.3
  338.2 2.3 copy-start.18
  341.9 3.8 copy-start.2
  343.4 3.6 copy-start.20
  344.4 2.6 copy-start.11
  344.4 2.6 copy-start.12
  344.4 2.6 copy-start.14
  344.4 2.6 copy-start.35
  345.7 3.0 copy-start.4
  348.6 0.9 copy-start.36
  348.6 1.0 copy-start.34
  348.6 1.0 copy-start.38
  348.6 1.0 copy-start.40
  348.6 1.5 copy-start.27
  348.6 1.5 copy-start.30
  348.7 1.5 copy-start.33
  354.3 13.4 %all-to-all-start.1 = ((bf16[4,2,16384]{2,1,0:T(2,128)(2,1)}), bf16[4,2,16384]{2,1,0:T(2,128)(2,1)S(1)}, u32[]{:S(2)}, u32[]{:S(2)}) async-start(bf16[4,2,16384]{2,1,0:T(2,128)(2,1)} %reshape.213), calls=%async_computation.1 | async-start | bytes 524288 | tf_op jit(solution)/shard_map/all_to_all | solution.py:113
  359.4 59.3 %all-reduce.13.cloned.1.call-start = ((), (), s32[]{:S(2)}) async-start(), calls=%async_computation.6 | async-start | bytes 267264 | tf_op jit(solution)/shard_map/psum | solution.py:107
  361.2 87.9 %all-gather.2.cloned.1.call-start = ((), (), s32[]{:S(2)}) async-start(), calls=%async_computation.4 | async-start | bytes 2359296 | tf_op jit(solution)/shard_map/all_gather | solution.py:115
  362.0 90.4 %reduce-scatter.2.cloned.1.call-start = ((), (), s32[]{:S(2)}) async-start(), calls=%async_computation.5 | async-start | bytes 655360 | tf_op jit(solution)/shard_map/reduce_scatter | solution.py:142
  400.3 1.4 copy-start.6
  400.6 1.3 copy-start.8
  400.6 1.3 copy-start.9
Sparse Core Ops, SparseCore 0:
  364.2 54.3 all-reduce.12
  420.6 28.4 all-gather.1
Sparse Core Ops, SparseCore 1:
  401.7 19.3 reduce-scatter.1
